TPU v7x, 32 devices: a whole 2x2x4 slice. The times are simulated.
32 devices in a mesh: ep: 4 (over y, x), tp: 8 (over z, core).
Axes of the slice: x: 2, y: 2, z: 4, core: 2. Of those that a mesh axis runs over, the one named last changes fastest.
Arguments:
- queries: bfloat16 [2048, 16, 128], P('ep', 'tp'), may hold values from -125 to 125
- keys: bfloat16 [2048, 16, 128], P('ep', 'tp'), may hold values from -9 to 9
- values: bfloat16 [2048, 16, 128], P('ep', 'tp'), may hold values from -6 to 6
- mixing: float32 [16], P('tp'), may hold values from 0.3 to 0.8
- head_gain: float32 [128], replicated, may hold values from 0.1 to 1.9
- out_weight: bfloat16 [16, 128, 2048], P('tp'), may hold values from -0.125 to 0.125
- tokens_b: bfloat16 [4096, 2048], P(('ep', 'tp')), may hold values from -6 to 6
- norm_gain: float32 [2048], replicated, may hold values from 0.1 to 1.9
- expert_ids: int32 [4096, 2], P(('ep', 'tp')), may hold values from 0 to 3, all different within a row; in each aligned block of 128 rows (0 to 127, 128 to 255, ...) at most 96 rows name the same one
- group_gate: float32 [4096], P(('ep', 'tp')), may hold values from 0.2 to 1
- expert_gate: float32 [4096, 2], P(('ep', 'tp')), may hold values from 0.1 to 0.9
- gate_weight: bfloat16 [4, 2048, 1024], P('ep', None, 'tp'), may hold values from -0.125 to 0.125
- up_weight: bfloat16 [4, 2048, 1024], P('ep', None, 'tp'), may hold values from -0.125 to 0.125
- down_weight: bfloat16 [4, 2048, 1024], P('ep', None, 'tp'), may hold values from -0.1875 to 0.1875
Outputs:
- mixed: bfloat16 [2048, 2048], P(('ep', 'tp'))
- routed: bfloat16 [4096, 2048], P(('ep', 'tp'))
Inputs may be any that keep to these rules, and one draw needn't show every extreme that they name: `expert_ids`: within each aligned block of 128 rows, no expert is named by more than 96 rows, and some block has an expert named by exactly 96 rows.
All inputs are finite; a program needn't handle non-finite values.
Results may differ from a plain program's by a relative error of at most 0.019.
Values may be sent and summed in bfloat16 or wider, within the bound.
A program may use at most 192 MiB of HBM per device.

v0:
```python
import math
import jax
import jax.numpy as jnp
from jax import lax
from jax.sharding import PartitionSpec as P

HEAD = 64


def attend_heads(queries, keys, values, mixing, head_gain):
    shard_rows = queries.shape[0]
    head_count = queries.shape[1]
    value_width = values.shape[2]
    query_start = lax.axis_index("ep") * shard_rows
    score_scale = 1.0 / math.sqrt(HEAD)
    query_pos = query_start + lax.iota(jnp.int32, shard_rows)

    def update(running, key_block, value_block, block_start):
        key_pos = block_start + lax.iota(jnp.int32, shard_rows)
        allowed = key_pos[None, :] <= query_pos[:, None]
        fresh = []
        for map_index in range(2):
            maximum, row_sum, numerator = running[3 * map_index : 3 * map_index + 3]
            offset = map_index * HEAD
            scores = (
                jnp.einsum(
                    "qhd,khd->hqk",
                    queries[:, :, offset : offset + HEAD],
                    key_block[:, :, offset : offset + HEAD],
                    preferred_element_type=jnp.float32,
                )
                * score_scale
            )
            scores = jnp.where(allowed[None], scores, -1e30)
            newmax = jnp.maximum(maximum, jnp.max(scores, axis=2))
            shrink = jnp.exp(maximum - newmax)
            weights = jnp.exp(scores - newmax[:, :, None])
            row_sum = row_sum * shrink + jnp.sum(weights, axis=2)
            numerator = numerator * shrink[:, :, None] + jnp.einsum(
                "hqk,khe->hqe",
                weights.astype(jnp.bfloat16),
                value_block,
                preferred_element_type=jnp.float32,
            )
            fresh += [newmax, row_sum, numerator]
        return tuple(fresh)

    floor_max = jnp.full((head_count, shard_rows), -1e30, jnp.float32)
    zero_sum = jnp.zeros((head_count, shard_rows), jnp.float32)
    zero_acc = jnp.zeros((head_count, shard_rows, value_width), jnp.float32)
    start_state = (floor_max, zero_sum, zero_acc, floor_max, zero_sum, zero_acc)
    running = start_state
    key_piece = lax.all_gather(keys, "ep", axis=0, tiled=True)
    value_piece = lax.all_gather(values, "ep", axis=0, tiled=True)
    blocks = key_piece.shape[0] // shard_rows
    key_blocks = key_piece.reshape(blocks, shard_rows, head_count, key_piece.shape[2])
    value_blocks = value_piece.reshape(blocks, shard_rows, head_count, value_width)

    def visit_block(state, inputs):
        key_block, value_block, block_index = inputs
        block_start = block_index * shard_rows
        state = lax.cond(
            block_start <= query_start + shard_rows - 1,
            lambda state_in: update(state_in, key_block, value_block, block_start),
            lambda state_in: state_in,
            state,
        )
        return (state, None)

    running, unused = lax.scan(
        visit_block, running, (key_blocks, value_blocks, lax.iota(jnp.int32, blocks))
    )
    state = running
    diff = state[2] / state[1][:, :, None] - mixing[:, None, None] * state[5] / state[4][:, :, None]
    normed = diff * lax.rsqrt(jnp.mean(diff * diff, axis=2, keepdims=True) + 1e-05) * head_gain
    return normed.astype(jnp.bfloat16)


def mixer_half(queries, keys, values, mixing, head_gain, out_weight):
    attended = attend_heads(queries, keys, values, mixing, head_gain)
    return lax.psum_scatter(
        jnp.einsum("hqe,hed->qd", attended, out_weight, preferred_element_type=jnp.float32).astype(
            jnp.bfloat16
        ),
        "tp",
        scatter_dimension=0,
        tiled=True,
    )


def expert_half(
    tokens_b, norm_gain, expert_ids, group_gate, expert_gate, gate_weight, up_weight, down_weight
):
    local_rows = tokens_b.shape[0]
    width = tokens_b.shape[1]
    top_count = expert_ids.shape[1]
    ep_count = lax.axis_size("ep")
    local_count = gate_weight.shape[0]
    expert_total = ep_count * local_count
    capacity = 3 * local_rows * top_count // (2 * expert_total)
    tokens_f = tokens_b.astype(jnp.float32)
    normed = (
        tokens_f
        * lax.rsqrt(jnp.mean(tokens_f * tokens_f, axis=1, keepdims=True) + 1e-06)
        * norm_gain
    ).astype(jnp.bfloat16)
    flat_ids = expert_ids.reshape(-1)
    one_hot = (flat_ids[:, None] == lax.iota(jnp.int32, expert_total)[None, :]).astype(jnp.int32)
    slot_rank = jnp.sum((jnp.cumsum(one_hot, axis=0) - one_hot) * one_hot, axis=1)
    slot_index = flat_ids * capacity + slot_rank
    owners = jnp.full((expert_total * capacity,), local_rows, jnp.int32)
    owners = owners.at[slot_index].set(lax.iota(jnp.int32, local_rows * top_count) // top_count)
    padded = jnp.concatenate([normed, jnp.zeros((1, width), jnp.bfloat16)], axis=0)
    outgoing = padded[owners].reshape(ep_count, local_count * capacity, width)
    incoming = lax.all_to_all(outgoing, "ep", split_axis=0, concat_axis=0, tiled=True)
    expert_rows = jnp.transpose(
        incoming.reshape(ep_count, local_count, capacity, width), (1, 0, 2, 3)
    )
    expert_rows = expert_rows.reshape(local_count, ep_count * capacity, width)
    piece_gate = lax.all_gather(gate_weight, "tp", axis=2, tiled=True)
    piece_up = lax.all_gather(up_weight, "tp", axis=2, tiled=True)
    piece_down = lax.all_gather(down_weight, "tp", axis=2, tiled=True)
    gate_part = jnp.einsum(
        "jrd,jdf->jrf", expert_rows, piece_gate, preferred_element_type=jnp.float32
    )
    up_part = jnp.einsum("jrd,jdf->jrf", expert_rows, piece_up, preferred_element_type=jnp.float32)
    hidden = (jax.nn.silu(gate_part) * up_part).astype(jnp.bfloat16)
    expert_out = jnp.einsum(
        "jrf,jdf->jrd", hidden, piece_down, preferred_element_type=jnp.float32
    ).astype(jnp.bfloat16)
    outbound = jnp.transpose(
        expert_out.reshape(local_count, ep_count, capacity, width), (1, 0, 2, 3)
    )
    outbound = outbound.reshape(ep_count, local_count * capacity, width)
    returned = lax.all_to_all(outbound, "ep", split_axis=0, concat_axis=0, tiled=True).reshape(
        expert_total * capacity, width
    )
    picked = returned[slot_index].reshape(local_rows, top_count, width).astype(jnp.float32)
    route_weight = group_gate[:, None] * expert_gate
    return jnp.sum(route_weight[:, :, None] * picked, axis=1).astype(jnp.bfloat16)


def per_device(
    queries,
    keys,
    values,
    mixing,
    head_gain,
    out_weight,
    tokens_b,
    norm_gain,
    expert_ids,
    group_gate,
    expert_gate,
    gate_weight,
    up_weight,
    down_weight,
):
    mixed = mixer_half(queries, keys, values, mixing, head_gain, out_weight)
    routed = expert_half(
        tokens_b,
        norm_gain,
        expert_ids,
        group_gate,
        expert_gate,
        gate_weight,
        up_weight,
        down_weight,
    )
    return (mixed, routed)


def solution(mesh):
    placed = (
        P("ep", "tp", None),
        P("ep", "tp", None),
        P("ep", "tp", None),
        P("tp"),
        P(),
        P("tp", None, None),
        P(("ep", "tp"), None),
        P(),
        P(("ep", "tp"), None),
        P(("ep", "tp")),
        P(("ep", "tp"), None),
        P("ep", None, "tp"),
        P("ep", None, "tp"),
        P("ep", None, "tp"),
    )
    return jax.shard_map(
        per_device,
        mesh=mesh,
        in_specs=placed,
        out_specs=(P(("ep", "tp"), None), P(("ep", "tp"), None)),
        check_vma=False,
    )
```

profile of v0, /device:TPU:0, one launch (start us, length us, event | category | flops | bytes accessed | tf_op | source)
XLA Modules:
  0.0 260.2 jit_solution(6079203360803837472)
XLA Ops:
  7.3 1.8 copy.24
  9.1 1.7 copy.25
  10.9 0.7 all-gather.10.cloned.1.call-update
  11.6 0.5 all-gather.12.cloned.1.call-update
  12.2 0.5 all-gather.14.cloned.1.call-update
  12.8 0.1 copy.31
  12.9 0.1 eq.29
  13.1 0.1 eq.25
  13.2 0.2 copy.27
  13.4 1.2 reduce-window.6
  14.7 0.1 copy.33
  15.0 0.1 copy.30
  15.1 0.1 mul.169
  15.3 1.4 scatter_custom_fusion
  16.7 0.2 fusion.31
  17.0 1.0 fusion.33
  17.9 21.8 %all-gather.6.cloned.1.call-done = bf16[2048,2,128]{2,0,1:T(8,128)(2,1)} async-done(((bf16[512,2,128]{2,0,1:T(8,128)(2,1)}), bf16[2048,2,128]{2,0,1:T(8,128)(2,1)}) %all-gather.6.cloned.1.call-update) | async-done | bytes 1048592 | tf_op jit(solution)/shard_map/all_gather | solution.py:53
  39.7 2.3 copy.26
  42.0 26.1 %all-gather.8.cloned.1.call-done = bf16[2048,2,128]{2,0,1:T(8,128)(2,1)} async-done(((bf16[512,2,128]{2,0,1:T(8,128)(2,1)}), bf16[2048,2,128]{2,0,1:T(8,128)(2,1)}) %all-gather.8.cloned.1.call-update) | async-done | bytes 1048592 | tf_op jit(solution)/shard_map/all_gather | solution.py:54
  68.1 1.3 copy.28
  69.5 9.8 %while.23 = (s32[]{:T(128)}, f32[2,512]{1,0:T(2,128)S(1)}, f32[2,512]{1,0:T(2,128)S(1)}, f32[2,512,128]{2,1,0:T(8,128)S(1)}, f32[2,512]{1,0:T(2,128)S(1)}, /*ind...) while((s32[]{:T(128)}, f32[2,512]{1,0:T(2,128)S(1)}, ...), condition=%wide.region_7.8_spmd.clone, body=%wide.region_0.7_spmd.clone.sunk | while | flops 410784768 | bytes 17183128 | solution.py:70
  69.6 0.6 dynamic_slice.36
  70.8 4.6 %conditional.3 = ((f32[2,512]{1,0:T(2,128)S(1)}, f32[2,512]{1,0:T(2,128)S(1)}, f32[2,512,128]{2,1,0:T(8,128)S(1)}, f32[2,512]{1,0:T(2,128)S(1)}, f32[2,512]{1,0:T(2,128)S(1)}, /*index=5*/f32[2,512,128]{2,1,0:T(8,128)S(1)})) conditional(s32[]{:T(128)} %convert_element_type.87, (f32[2,512]{1,0:T(2,128)S(1)}, f32[2,512]{1,0:T(2,128)S(1)}, ...), branch_computations={%region_1.1_spmd, %region_2.6_spmd} | conditional | flops 410784768 | bytes 17180748 | solution.py:62
  70.8 1.0 dynamic-slice_bitcast_fusion
  71.8 0.2 broadcast_compare_fusion
  72.1 0.6 fusion.45
  72.7 0.3 fusion.3
  73.0 0.6 fusion.46
  73.6 0.3 fusion.5
  74.0 0.7 convolution_add_fusion
  74.7 0.7 convolution_add_fusion.1
  75.5 0.6 dynamic_slice.36
  76.8 0.6 dynamic_slice.36
  78.1 0.6 dynamic_slice.36
  79.4 0.5 multiply_reduce_fusion.1
  79.9 2.1 bitcast_convert_fusion
  82.2 2.5 gather_fusion
  84.6 36.1 %all_to_all.10 = bf16[4,96,2048]{2,1,0:T(8,128)(2,1)} all-to-all(bf16[4,96,2048]{2,1,0:T(8,128)(2,1)S(1)} %bitcast.62), channel_id=1, replica_groups=mesh['ep'=4,'tp'=8] {'ep'}, dimensions={0} | all-to-all | bytes 3145728 | tf_op jit(solution)/shard_map/all_to_all | solution.py:115
  120.7 5.7 %fusion.24 = f32[384,1024]{1,0:T(8,128)} fusion(bf16[384,2048]{1,0:T(8,128)(2,1)} %bitcast.63, bf16[1,2048,1024]{2,1,0:T(8,128)(2,1)} %all-gather.10.cloned.1.call-done), kind=kOutput, calls=%fused_computation.38 | convolution fusion | flops 1610612736 | bytes 7340032 | tf_op jit(solution)/shard_map/jrd,jdf->jrf/dot_general | solution.py:123
  126.4 38.6 %all-gather.12.cloned.1.call-done = bf16[1,2048,1024]{2,1,0:T(8,128)(2,1)} async-done(((bf16[1,2048,128]{2,1,0:T(8,128)(2,1)}), bf16[1,2048,1024]{2,1,0:T(8,128)(2,1)}) %all-gather.12.cloned.1.call-update) | async-done | bytes 4194320 | tf_op jit(solution)/shard_map/all_gather | solution.py:121
  165.0 47.5 %all-gather.14.cloned.1.call-done = bf16[1,2048,1024]{2,1,0:T(8,128)(2,1)} async-done(((bf16[1,2048,128]{2,1,0:T(8,128)(2,1)}), bf16[1,2048,1024]{2,1,0:T(8,128)(2,1)}) %all-gather.14.cloned.1.call-update) | async-done | bytes 4194320 | tf_op jit(solution)/shard_map/all_gather | solution.py:122
  212.5 8.6 %fusion.26 = bf16[384,2048]{1,0:T(8,128)(2,1)} fusion(bf16[1,2048,1024]{2,1,0:T(8,128)(2,1)} %all-gather.14.cloned.1.call-done, f32[384,1024]{1,0:T(8,128)} %fusion.24, bf16[384,2048]{1,0:T(8,128)(2,1)S(1)} %bitcast.64, bf16[1,2048,1024]{2,1,0:T(8,128)(2,1)} %all-gather.12.cloned.1.call-done), kind=kOutput, calls=%fused_computation.41 | convolution fusion | flops 3224371200 | bytes 13107200 | tf_op jit(solution)/shard_map/jrf,jdf->jrd/dot_general | solution.py:128
  221.1 3.8 %all-to-all-start.1 = ((bf16[4,96,2048]{2,1,0:T(8,128)(2,1)}), bf16[4,96,2048]{2,1,0:T(8,128)(2,1)S(1)}, u32[]{:S(2)}, u32[]{:S(2)}) async-start(bf16[4,96,2048]{2,1,0:T(8,128)(2,1)} %bitcast.65), calls=%async_computation.2 | async-start | bytes 3145728 | tf_op jit(solution)/shard_map/all_to_all | solution.py:135
  224.9 0.1 copy.29
  225.0 19.7 %all-to-all-done.1 = bf16[4,96,2048]{2,1,0:T(8,128)(2,1)S(1)} async-done(((bf16[4,96,2048]{2,1,0:T(8,128)(2,1)}), bf16[4,96,2048]{2,1,0:T(8,128)(2,1)S(1)}, u32[]{:S(2)}, u32[]{:S(2)}) %all-to-all-start.1) | async-done | bytes 1572896 | tf_op jit(solution)/shard_map/all_to_all | solution.py:135
  244.7 2.3 gather_fusion.1
  247.1 2.4 reshape.163
  249.4 3.9 %multiply_reduce_fusion = bf16[128,2048]{1,0:T(8,128)(2,1)} fusion(f32[128,2,2048]{2,1,0:T(2,128)S(1)} %reshape.163, f32[128,2]{1,0:T(8,128)S(1)} %copy.29), kind=kLoop, calls=%fused_computation.42 | loop fusion | flops 786432 | bytes 2622464 | tf_op jit(solution)/shard_map/reduce_sum | solution.py:140
  (71 shorter events, 1.0 us)
Async XLA Ops:
  7.2 72.7 %copy-start = (bf16[2,128,2048]{2,1,0:T(8,128)(2,1)S(1)}, bf16[2,128,2048]{2,1,0:T(8,128)(2,1)}, u32[]{:S(2)}) copy-start(bf16[2,128,2048]{2,1,0:T(8,128)(2,1)} %param.23) | copy-start | bytes 3145732
  7.2 5.6 %copy-start.6 = (s32[128,2]{0,1:T(2,128)S(1)}, s32[128,2]{0,1:T(2,128)}, u32[]{:S(2)}) copy-start(s32[128,2]{0,1:T(2,128)} %param.26) | copy-start | bytes 3076
  7.2 6.0 %copy-start.4 = (bf16[512,2,128]{2,1,0:T(2,128)(2,1)S(1)}, bf16[512,2,128]{2,1,0:T(2,128)(2,1)}, u32[]{:S(2)}) copy-start(bf16[512,2,128]{2,1,0:T(2,128)(2,1)} %param.18) | copy-start | bytes 786436
  7.2 9.5 %copy-start.1 = (bf16[128,2048]{1,0:T(8,128)(2,1)S(1)}, bf16[128,2048]{1,0:T(8,128)(2,1)}, u32[]{:S(2)}) copy-start(bf16[128,2048]{1,0:T(8,128)(2,1)} %param.24) | copy-start | bytes 1572868
  7.2 32.5 %all-gather.6.cloned.1.call-start = ((), (), s32[]{:S(2)}) async-start(), calls=%async_computation.3 | async-start | bytes 1310720 | tf_op jit(solution)/shard_map/all_gather | solution.py:53
  9.1 7.9 %copy-start.5 = (f32[2048]{0:T(1024)S(1)}, f32[2048]{0:T(1024)}, u32[]{:S(2)}) copy-start(f32[2048]{0:T(1024)} %param.25) | copy-start | bytes 24580
  9.1 59.0 %all-gather.8.cloned.1.call-start = ((), (), s32[]{:S(2)}) async-start(), calls=%async_computation.4 | async-start | bytes 1310720 | tf_op jit(solution)/shard_map/all_gather | solution.py:54
  10.8 109.8 %all-gather.10.cloned.1.call-start = ((), (), s32[]{:S(2)}) async-start(), calls=%async_computation.6 | async-start | bytes 4718592 | tf_op jit(solution)/shard_map/all_gather | solution.py:120
  11.6 153.4 %all-gather.12.cloned.1.call-start = ((), (), s32[]{:S(2)}) async-start(), calls=%async_computation.7 | async-start | bytes 4718592 | tf_op jit(solution)/shard_map/all_gather | solution.py:121
  12.2 200.3 %all-gather.14.cloned.1.call-start = ((), (), s32[]{:S(2)}) async-start(), calls=%async_computation.8 | async-start | bytes 4718592 | tf_op jit(solution)/shard_map/all_gather | solution.py:122
  12.7 240.6 %reduce-scatter.2.cloned.1.call-start = ((), (), s32[]{:S(2)}) async-start(), calls=%async_computation.5 | async-start | bytes 2359296 | tf_op jit(solution)/shard_map/reduce_scatter | solution.py:81
  69.5 9.9 %copy-start.8 = (f32[2]{0:T(128)S(1)}, f32[2]{0:T(128)}, u32[]{:S(2)}) copy-start(f32[2]{0:T(128)} %param.21) | copy-start | bytes 28
  69.5 10.4 %copy-start.9 = (f32[128]{0:T(128)S(1)}, f32[128]{0:T(128)}, u32[]{:S(2)}) copy-start(f32[128]{0:T(128)} %param.22) | copy-start | bytes 1540
  79.9 2.2 copy-start.2
  120.7 91.8 %copy-start.3 = (bf16[4,96,2048]{2,1,0:T(8,128)(2,1)S(1)}, bf16[4,96,2048]{2,1,0:T(8,128)(2,1)}, u32[]{:S(2)}) copy-start(bf16[4,96,2048]{2,1,0:T(8,128)(2,1)} %all_to_all.10) | copy-start | bytes 4718596
  221.1 3.8 %copy-start.7 = (f32[128,2]{0,1:T(2,128)S(1)}, f32[128,2]{0,1:T(2,128)}, u32[]{:S(2)}) copy-start(f32[128,2]{0,1:T(2,128)} %param.28) | copy-start | bytes 3076
  221.1 3.8 %copy-start.10 = (f32[128]{0:T(128)S(1)}, f32[128]{0:T(128)}, u32[]{:S(2)}) copy-start(f32[128]{0:T(128)} %param.27) | copy-start | bytes 1540
  221.1 23.6 %all-to-all-start.1 = ((bf16[4,96,2048]{2,1,0:T(8,128)(2,1)}), bf16[4,96,2048]{2,1,0:T(8,128)(2,1)S(1)}, u32[]{:S(2)}, u32[]{:S(2)}) async-start(bf16[4,96,2048]{2,1,0:T(8,128)(2,1)} %bitcast.65), calls=%async_computation.2 | async-start | bytes 3145728 | tf_op jit(solution)/shard_map/all_to_all | solution.py:135
Sparse Core Ops, SparseCore 0:
  10.4 29.2 all-gather.5
  41.5 26.4 all-gather.7
  69.7 47.8 all-gather.9
  119.0 45.9 all-gather.11
  166.4 45.9 all-gather.13
  215.2 34.1 reduce-scatter.1
where the time goes:
time: 261 us; the launch traced here: 260 us
  waiting for transfers between devices  155 us (59%)
  blocking collectives  36.1 us (14%)
  local copies, waits for them, and re-layouts  20.4 us (8%)
  matrix products  19.2 us (7%)
  between operations  14.4 us (6%)
  other arithmetic  7.89 us (3%)
  starting transfers between devices  4.02 us (2%)
  loops' own time  2.93 us (1%)
    all_gather x1, waiting for transfers between devices, expert_half(): piece_down = lax.all_gather(down_weight, 'tp', axis=2, tiled=True)  47.5 us
    all_gather x1, waiting for transfers between devices, expert_half(): piece_up = lax.all_gather(up_weight, 'tp', axis=2, tiled=True)  38.6 us
    all_to_all x1, blocking collectives, expert_half(): lax.all_to_all(outgoing, 'ep', split_axis=0, concat_axis=0, tiled=True)  36.1 us
    all_gather x1, waiting for transfers between devices, attend_heads(): value_piece = lax.all_gather(values, 'ep', axis=0, tiled=True)  26.1 us
    all_gather x1, waiting for transfers between devices, attend_heads(): key_piece = lax.all_gather(keys, 'ep', axis=0, tiled=True)  21.8 us
    all_to_all x1, waiting for transfers between devices, expert_half(): lax.all_to_all(outbound, 'ep', split_axis=0, concat_axis=0, tiled=True)  19.7 us
    dot_general x1, matrix products, expert_half(): jnp.einsum('jrf,jdf->jrd', hidden, piece_down, preferred_element_type=jnp...  8.63 us
    unnamed x28, local copies, waits for them, and re-layouts  7.42 us
  transfers between devices with their start and end apart: 7, of which 5 were waited for; matrix products, arithmetic and copies ran while one was open for 18% of the time, Pallas kernels for 0%

commit v1 on v0

--- a/solution.py
+++ b/solution.py
@@ -5,6 +5,32 @@
 from jax.sharding import PartitionSpec as P
 
 HEAD = 64
+
+
+def ring_apply(x, axis, dim, work, out_dim):
+    size, index, extent = (lax.axis_size(axis), lax.axis_index(axis), x.shape[dim])
+    ahead = [(i, (i + 1) % size) for i in range(size)]
+    downward = [(b, a) for a, b in ahead]
+    lower, upper = (lax.ppermute(x, axis, ahead), lax.ppermute(x, axis, downward))
+    made = work(x, index * extent)
+    length = made.shape[out_dim]
+    result = jnp.zeros(
+        (*made.shape[:out_dim], size * length, *made.shape[out_dim + 1 :]), made.dtype
+    )
+
+    def put(result, made, owner):
+        return lax.dynamic_update_slice_in_dim(result, made, owner * length, axis=out_dim)
+
+    result = put(result, made, index)
+    for step in range(1, size // 2 + 1):
+        below, above = ((index - step) % size, (index + step) % size)
+        block = (lower, upper)
+        if step < size // 2:
+            lower, upper = (lax.ppermute(lower, axis, ahead), lax.ppermute(upper, axis, downward))
+        result = put(result, work(block[0], below * extent), below)
+        if 2 * step < size:
+            result = put(result, work(block[1], above * extent), above)
+    return result
 
 
 def attend_heads(queries, keys, values, mixing, head_gain):
@@ -118,12 +144,19 @@
     )
     expert_rows = expert_rows.reshape(local_count, ep_count * capacity, width)
     piece_gate = lax.all_gather(gate_weight, "tp", axis=2, tiled=True)
-    piece_up = lax.all_gather(up_weight, "tp", axis=2, tiled=True)
     piece_down = lax.all_gather(down_weight, "tp", axis=2, tiled=True)
     gate_part = jnp.einsum(
         "jrd,jdf->jrf", expert_rows, piece_gate, preferred_element_type=jnp.float32
     )
-    up_part = jnp.einsum("jrd,jdf->jrf", expert_rows, piece_up, preferred_element_type=jnp.float32)
+    up_part = ring_apply(
+        up_weight,
+        "tp",
+        2,
+        lambda part, offset_2: jnp.einsum(
+            "jrd,jdf->jrf", expert_rows, part, preferred_element_type=jnp.float32
+        ),
+        2,
+    )
     hidden = (jax.nn.silu(gate_part) * up_part).astype(jnp.bfloat16)
     expert_out = jnp.einsum(
         "jrf,jdf->jrd", hidden, piece_down, preferred_element_type=jnp.float32

time: 261 us -> 231 us (0.89)
  blocking collectives: 36.1 us -> 0 us
  waiting for transfers between devices: 155 us -> 127 us
  starting transfers between devices: 4.02 us -> 19.9 us
  matrix products: 19.2 us -> 29.8 us
  local copies, waits for them, and re-layouts: 20.4 us -> 27.1 us
    all_gather x1, waiting for transfers between devices: 0.01 us -> 46 us  [expert_half(): piece_gate = lax.all_gather(gate_weight, 'tp', axis=2, tiled=True)]
    all_gather x1, waiting for transfers between devices: 47.5 us -> 4.85 us  [expert_half(): piece_down = lax.all_gather(down_weight, 'tp', axis=2, tiled=True)]
    all_gather x1 -> x0, waiting for transfers between devices: 38.6 us -> none  [expert_half(): piece_up = lax.all_gather(up_weight, 'tp', axis=2, tiled=True)]
    ppermute x0 -> x7, waiting for transfers between devices: none -> 37.1 us  [the longest x3 26.6 us: ring_apply(): lax.ppermute(lower, axis, ahead)]
    all_to_all x1 -> x0, blocking collectives: 36.1 us -> none  [expert_half(): lax.all_to_all(outgoing, 'ep', split_axis=0, concat_axis=0, tiled=True)]
    all_gather x1, waiting for transfers between devices: 21.8 us -> 0.01 us  [attend_heads(): key_piece = lax.all_gather(keys, 'ep', axis=0, tiled=True)]
    dot_general x1 -> x8, matrix products: 5.74 us -> 16.4 us  [expert_half(): jnp.einsum('jrd,jdf->jrf', expert_rows, part, preferred_element_type=jnp....]
    ppermute x0 -> x7, starting transfers between devices: none -> 10.7 us  [the longest x2 7.08 us: ring_apply(): lax.ppermute(upper, axis, downward)]
  transfers between devices with their start and end apart: 7 -> 14, of which waited for: 5 -> 7; matrix products, arithmetic and copies ran while one was open for 18% -> 28% of each run, Pallas kernels for 0% -> 0%
where the time goes in v1:
time: 231 us; the launch traced here: 230 us
  waiting for transfers between devices  127 us (55%)
  matrix products  29.8 us (13%)
  local copies, waits for them, and re-layouts  27.1 us (12%)
  starting transfers between devices  19.9 us (9%)
  between operations  14 us (6%)
  other arithmetic  9.8 us (4%)
  loops' own time  2.9 us (1%)
    all_gather x1, waiting for transfers between devices, expert_half(): piece_gate = lax.all_gather(gate_weight, 'tp', axis=2, tiled=True)  46 us
    ppermute x3, waiting for transfers between devices, ring_apply(): lax.ppermute(lower, axis, ahead)  26.6 us
    all_to_all x1, waiting for transfers between devices, expert_half(): lax.all_to_all(outbound, 'ep', split_axis=0, concat_axis=0, tiled=True)  19.7 us
    all_gather x1, waiting for transfers between devices, attend_heads(): value_piece = lax.all_gather(values, 'ep', axis=0, tiled=True)  17.9 us
    dot_general x8, matrix products, expert_half(): jnp.einsum('jrd,jdf->jrf', expert_rows, part, preferred_element_type=jnp....  16.4 us
    ppermute x1, waiting for transfers between devices, ring_apply(): lax.ppermute(x, axis, ahead)  10.5 us
    unnamed x28, local copies, waits for them, and re-layouts  9.17 us
    dot_general x1, matrix products, expert_half(): jnp.einsum('jrf,jdf->jrd', hidden, piece_down, preferred_element_type=jnp...  8.58 us
  transfers between devices with their start and end apart: 14, of which 7 were waited for; matrix products, arithmetic and copies ran while one was open for 28% of the time, Pallas kernels for 0%

profile of v1, /device:TPU:0, one launch (start us, length us, event | category | flops | bytes accessed | tf_op | source)
XLA Modules:
  0.0 230.3 jit_solution(11280290162226269101)
XLA Ops:
  7.2 1.8 copy.24
  9.1 1.7 copy.25
  10.9 0.7 all-gather.11.cloned.1.call-update
  12.6 1.2 reduce-window.6
  15.0 1.4 scatter_custom_fusion
  16.4 3.1 %gather_fusion = bf16[384,2048]{1,0:T(8,128)(2,1)} fusion(bf16[129,2048]{1,0:T(8,128)(2,1)S(1)} %concatenate.3, s32[1024]{0:T(1024)S(1)} %pad_clamp_fusion.1), kind=kCustom, calls=%fused_computation | custom fusion | bytes 3147264 | tf_op jit(solution)/shard_map/gather | solution.py:140
  19.5 5.3 %all-to-all-start = ((bf16[4,96,2048]{2,1,0:T(8,128)(2,1)}), bf16[4,96,2048]{2,1,0:T(8,128)(2,1)S(1)}, u32[]{:S(2)}, u32[]{:S(2)}) async-start(bf16[4,96,2048]{2,1,0:T(8,128)(2,1)} %bitcast.145), calls=%async_computation.1 | async-start | bytes 3145728 | tf_op jit(solution)/shard_map/all_to_all | solution.py:141
  24.9 3.5 %collective-permute-start.1 = (bf16[1,2048,128]{2,1,0:T(8,128)(2,1)S(1)}, bf16[1,2048,128]{2,1,0:T(8,128)(2,1)}, u32[]{:S(2)}, u32[]{:S(2)}) collective-permute-start(bf16[1,2048,128]{2,1,0:T(8,128)(2,1)S(1)} %copy-done.5), channel_id=1, source_target_pairs={{1,0},{2,1},{3,2},{4,3},{5,4},{6,5},{7,6},{0,7},{9,8},{10,9},{11,1... | collective-permute-start | bytes 1572872 | tf_op jit(solution)/shard_map/ppermute | solution.py:14
  28.4 10.5 %collective-permute-done = bf16[1,2048,128]{2,1,0:T(8,128)(2,1)} collective-permute-done((bf16[1,2048,128]{2,1,0:T(8,128)(2,1)S(1)}, bf16[1,2048,128]{2,1,0:T(8,128)(2,1)}, u32[]{:S(2)}, u32[]{:S(2)}) %collective-permute-start) | collective-permute-done | bytes 524320 | tf_op jit(solution)/shard_map/ppermute | solution.py:14
  38.9 3.5 %collective-permute-start.3 = (bf16[1,2048,128]{2,1,0:T(8,128)(2,1)}, bf16[1,2048,128]{2,1,0:T(8,128)(2,1)}, u32[]{:S(2)}, u32[]{:S(2)}) collective-permute-start(bf16[1,2048,128]{2,1,0:T(8,128)(2,1)} %collective-permute-done.1), channel_id=1, source_target_pairs={{1,0},{2,1},{3,2},{4,3},{5,4},{6,5},{7,6},{0,7},{9,8},{10,9},{11,1... | collective-permute-start | bytes 1572872 | tf_op jit(solution)/shard_map/ppermute | solution.py:29
  42.5 0.9 copy.27
  43.3 9.5 %collective-permute-done.2 = bf16[1,2048,128]{2,1,0:T(8,128)(2,1)} collective-permute-done((bf16[1,2048,128]{2,1,0:T(8,128)(2,1)}, bf16[1,2048,128]{2,1,0:T(8,128)(2,1)}, u32[]{:S(2)}, u32[]{:S(2)}) %collective-permute-start.2) | collective-permute-done | bytes 524320 | tf_op jit(solution)/shard_map/ppermute | solution.py:29
  52.8 3.5 %collective-permute-start.5 = (bf16[1,2048,128]{2,1,0:T(8,128)(2,1)}, bf16[1,2048,128]{2,1,0:T(8,128)(2,1)}, u32[]{:S(2)}, u32[]{:S(2)}) collective-permute-start(bf16[1,2048,128]{2,1,0:T(8,128)(2,1)} %collective-permute-done.3), channel_id=1, source_target_pairs={{1,0},{2,1},{3,2},{4,3},{5,4},{6,5},{7,6},{0,7},{9,8},{10,9},{11,1... | collective-permute-start | bytes 1572872 | tf_op jit(solution)/shard_map/ppermute | solution.py:29
  56.4 1.4 broadcast_in_dim.65
  57.8 1.3 fusion.40
  59.0 2.3 %copy.26 = bf16[4,512,2,128]{1,3,2,0:T(8,128)(2,1)} copy(bf16[4,512,2,128]{3,1,0,2:T(8,128)(2,1)} %bitcast.147) | data formatting | bytes 2097152
  61.4 17.9 %all-gather.7.cloned.1.call-done = bf16[2048,2,128]{2,0,1:T(8,128)(2,1)} async-done(((bf16[512,2,128]{2,0,1:T(8,128)(2,1)}), bf16[2048,2,128]{2,0,1:T(8,128)(2,1)}) %all-gather.7.cloned.1.call-update) | async-done | bytes 1048592 | tf_op jit(solution)/shard_map/all_gather | solution.py:80
  79.3 2.3 %copy.28 = bf16[4,512,2,128]{3,1,2,0:T(8,128)(2,1)} copy(bf16[4,512,2,128]{3,1,0,2:T(8,128)(2,1)} %bitcast.148) | data formatting | bytes 2097152
  81.6 0.8 broadcast_in_dim.62.clone
  82.5 11.0 %while.23 = (s32[]{:T(128)}, f32[2,512]{1,0:T(2,128)S(1)}, f32[2,512]{1,0:T(2,128)S(1)}, f32[2,512,128]{2,1,0:T(8,128)S(1)}, f32[2,512]{1,0:T(2,128)S(1)}, /*ind...) while((s32[]{:T(128)}, f32[2,512]{1,0:T(2,128)S(1)}, ...), condition=%wide.region_7.8_spmd.clone, body=%wide.region_0.7_spmd.clone.sunk | while | flops 410784768 | bytes 25571820 | solution.py:96
  82.5 0.6 dynamic_slice.36
  83.8 5.8 %conditional.3 = ((f32[2,512]{1,0:T(2,128)S(1)}, f32[2,512]{1,0:T(2,128)S(1)}, f32[2,512,128]{2,1,0:T(8,128)S(1)}, f32[2,512]{1,0:T(2,128)S(1)}, f32[2,512]{1,0:T(2,128)S(1)}, /*index=5*/f32[2,512,128]{2,1,0:T(8,128)})) conditional(s32[]{:T(128)} %convert_element_type.88, (f32[2,512]{1,0:T(2,128)S(1)}, f32[2,512]{1,0:T(2,128)S(1)}, ...), branch_computations={%region_1.1_spmd, %region_2.6_spmd} | conditional | flops 410784768 | bytes 25569440 | solution.py:88
  83.8 1.0 dynamic-slice_bitcast_fusion
  85.0 0.6 fusion.63
  86.0 0.6 fusion.64
  87.0 0.7 copy-done.1
  88.1 0.7 convolution_add_fusion
  88.8 0.7 convolution_add_fusion.1
  90.9 0.6 dynamic_slice.36
  92.2 0.6 dynamic_slice.36
  93.5 1.6 multiply_reduce_fusion.1
  95.1 2.1 bitcast_convert_fusion
  97.2 2.3 %fusion.39 = f32[1,384,1024]{2,1,0:T(8,128)} fusion(f32[1,384,1024]{2,1,0:T(8,128)} %fusion.40, s32[]{:T(128)S(6)} %select_n.90, bf16[384,2048]{1,0:T(8,128)(2,1)S(1)} %bitcast.136, bf16[1,2048,128]{2,1,0:T(8,128)(2,1)} %collective-permute-done), kind=kOutput, calls=%fused_computation.59 | convolution fusion | flops 201326592 | bytes 2293764 | tf_op jit(solution)/shard_map/jrd,jdf->jrf/dot_general | solution.py:155
  99.5 2.3 %fusion.38 = f32[1,384,1024]{2,1,0:T(8,128)} fusion(f32[1,384,1024]{2,1,0:T(8,128)} %fusion.39, s32[]{:T(128)S(6)} %select_n.92, bf16[384,2048]{1,0:T(8,128)(2,1)S(1)} %bitcast.137, bf16[1,2048,128]{2,1,0:T(8,128)(2,1)} %collective-permute-done.1), kind=kOutput, calls=%fused_computation.57 | convolution fusion | flops 201326592 | bytes 2293764 | tf_op jit(solution)/shard_map/jrd,jdf->jrf/dot_general | solution.py:155
  101.8 2.3 fusion.37
  104.1 2.3 %fusion.36 = f32[1,384,1024]{2,1,0:T(8,128)} fusion(f32[1,384,1024]{2,1,0:T(8,128)} %fusion.37, s32[]{:T(128)S(6)} %select_n.96, bf16[384,2048]{1,0:T(8,128)(2,1)S(1)} %bitcast.139, bf16[1,2048,128]{2,1,0:T(8,128)(2,1)} %collective-permute-done.3), kind=kOutput, calls=%fused_computation.53 | convolution fusion | flops 201326592 | bytes 2293764 | tf_op jit(solution)/shard_map/jrd,jdf->jrf/dot_general | solution.py:155
  106.4 2.3 %fusion.35 = f32[1,384,1024]{2,1,0:T(8,128)} fusion(f32[1,384,1024]{2,1,0:T(8,128)} %fusion.36, s32[]{:T(128)S(6)} %select_n.98, bf16[384,2048]{1,0:T(8,128)(2,1)S(1)} %bitcast.140, bf16[1,2048,128]{2,1,0:T(8,128)(2,1)} %collective-permute-done.4), kind=kOutput, calls=%fused_computation.51 | convolution fusion | flops 201326592 | bytes 2293764 | tf_op jit(solution)/shard_map/jrd,jdf->jrf/dot_general | solution.py:155
  108.8 2.3 %fusion.34 = f32[1,384,1024]{2,1,0:T(8,128)} fusion(f32[1,384,1024]{2,1,0:T(8,128)} %fusion.35, s32[]{:T(128)S(6)} %select_n.100, bf16[384,2048]{1,0:T(8,128)(2,1)S(1)} %bitcast.141, bf16[1,2048,128]{2,1,0:T(8,128)(2,1)} %collective-permute-done.5), kind=kOutput, calls=%fused_computation.49 | convolution fusion | flops 201326592 | bytes 2293764 | tf_op jit(solution)/shard_map/jrd,jdf->jrf/dot_general | solution.py:155
  111.1 17.1 %collective-permute-done.6 = bf16[1,2048,128]{2,1,0:T(8,128)(2,1)S(1)} collective-permute-done((bf16[1,2048,128]{2,1,0:T(8,128)(2,1)}, bf16[1,2048,128]{2,1,0:T(8,128)(2,1)S(1)}, u32[]{:S(2)}, u32[]{:S(2)}) %collective-permute-start.6) | collective-permute-done | bytes 524320 | tf_op jit(solution)/shard_map/ppermute | solution.py:29
  128.1 1.3 fusion.33
  129.4 4.9 %all-gather.11.cloned.1.call-done = bf16[1,2048,1024]{2,1,0:T(8,128)(2,1)} async-done(((bf16[1,2048,128]{2,1,0:T(8,128)(2,1)}), bf16[1,2048,1024]{2,1,0:T(8,128)(2,1)}) %all-gather.11.cloned.1.call-update) | async-done | bytes 4194320 | tf_op jit(solution)/shard_map/all_gather | solution.py:147
  134.3 46.0 %all-gather.9.cloned.1.call-done = bf16[1,2048,1024]{2,1,0:T(8,128)(2,1)} async-done(((bf16[1,2048,128]{2,1,0:T(8,128)(2,1)}), bf16[1,2048,1024]{2,1,0:T(8,128)(2,1)}) %all-gather.9.cloned.1.call-update) | async-done | bytes 4194320 | tf_op jit(solution)/shard_map/all_gather | solution.py:146
  180.3 8.6 %fusion.24 = bf16[384,2048]{1,0:T(8,128)(2,1)} fusion(bf16[1,2048,1024]{2,1,0:T(8,128)(2,1)} %all-gather.11.cloned.1.call-done, f32[1,384,1024]{2,1,0:T(8,128)} %fusion.33, bf16[384,2048]{1,0:T(8,128)(2,1)S(1)} %bitcast.143, bf16[1,2048,1024]{2,1,0:T(8,128)(2,1)} %all-gather.9.cloned.1.call-done), kind=kOutput, calls=%fused_computation.39 | convolution fusion | flops 3224371200 | bytes 13107200 | tf_op jit(solution)/shard_map/jrf,jdf->jrd/dot_general | solution.py:161
  188.9 3.8 %all-to-all-start.1 = ((bf16[4,96,2048]{2,1,0:T(8,128)(2,1)}), bf16[4,96,2048]{2,1,0:T(8,128)(2,1)S(1)}, u32[]{:S(2)}, u32[]{:S(2)}) async-start(bf16[4,96,2048]{2,1,0:T(8,128)(2,1)} %bitcast.146), calls=%async_computation.2 | async-start | bytes 3145728 | tf_op jit(solution)/shard_map/all_to_all | solution.py:168
  192.8 19.7 %all-to-all-done.1 = bf16[4,96,2048]{2,1,0:T(8,128)(2,1)S(1)} async-done(((bf16[4,96,2048]{2,1,0:T(8,128)(2,1)}), bf16[4,96,2048]{2,1,0:T(8,128)(2,1)S(1)}, u32[]{:S(2)}, u32[]{:S(2)}) %all-to-all-start.1) | async-done | bytes 1572896 | tf_op jit(solution)/shard_map/all_to_all | solution.py:168
  212.5 2.3 %gather_fusion.1 = bf16[256,2048]{1,0:T(8,128)(2,1)} fusion(bf16[384,2048]{1,0:T(8,128)(2,1)S(1)} %bitcast.144, s32[1024]{0:T(1024)S(1)} %pad_clamp_fusion), kind=kCustom, calls=%fused_computation.1 | custom fusion | bytes 2098176 | tf_op jit(solution)/shard_map/gather | solution.py:171
  214.8 3.4 %reshape.212 = f32[128,2,2048]{2,1,0:T(2,128)} reshape(bf16[256,2048]{1,0:T(8,128)(2,1)} %gather_fusion.1) | data formatting | bytes 3145728 | tf_op jit(solution)/shard_map/convert_element_type | solution.py:171
  218.2 5.6 %multiply_reduce_fusion = bf16[128,2048]{1,0:T(8,128)(2,1)} fusion(f32[128,2,2048]{2,1,0:T(2,128)} %reshape.212, f32[128,2]{1,0:T(8,128)S(1)} %copy.29), kind=kLoop, calls=%fused_computation.40 | loop fusion | flops 786432 | bytes 2622464 | tf_op jit(solution)/shard_map/reduce_sum | solution.py:173
  (97 shorter events, 4.5 us)
Async XLA Ops:
  7.2 87.9 %copy-start = (bf16[2,128,2048]{2,1,0:T(8,128)(2,1)S(1)}, bf16[2,128,2048]{2,1,0:T(8,128)(2,1)}, u32[]{:S(2)}) copy-start(bf16[2,128,2048]{2,1,0:T(8,128)(2,1)} %param.23) | copy-start | bytes 3145732
  7.2 5.0 %copy-start.9 = (s32[128,2]{0,1:T(2,128)S(1)}, s32[128,2]{0,1:T(2,128)}, u32[]{:S(2)}) copy-start(s32[128,2]{0,1:T(2,128)} %param.26) | copy-start | bytes 3076
  7.2 7.2 %copy-start.4 = (bf16[128,2048]{1,0:T(8,128)(2,1)S(1)}, bf16[128,2048]{1,0:T(8,128)(2,1)}, u32[]{:S(2)}) copy-start(bf16[128,2048]{1,0:T(8,128)(2,1)} %param.24) | copy-start | bytes 1572868
  7.2 51.8 %all-gather.5.cloned.1.call-start = ((), (), s32[]{:S(2)}) async-start(), calls=%async_computation.3 | async-start | bytes 1310720 | tf_op jit(solution)/shard_map/all_gather | solution.py:79
  9.0 5.5 %copy-start.8 = (f32[2048]{0:T(1024)S(1)}, f32[2048]{0:T(1024)}, u32[]{:S(2)}) copy-start(f32[2048]{0:T(1024)} %param.25) | copy-start | bytes 24580
  9.1 70.2 %all-gather.7.cloned.1.call-start = ((), (), s32[]{:S(2)}) async-start(), calls=%async_computation.4 | async-start | bytes 1310720 | tf_op jit(solution)/shard_map/all_gather | solution.py:80
  10.8 123.5 %all-gather.11.cloned.1.call-start = ((), (), s32[]{:S(2)}) async-start(), calls=%async_computation.7 | async-start | bytes 4718592 | tf_op jit(solution)/shard_map/all_gather | solution.py:147
  11.6 168.7 %all-gather.9.cloned.1.call-start = ((), (), s32[]{:S(2)}) async-start(), calls=%async_computation.6 | async-start | bytes 4718592 | tf_op jit(solution)/shard_map/all_gather | solution.py:146
  19.5 5.3 %copy-start.5 = (bf16[1,2048,128]{2,1,0:T(8,128)(2,1)S(1)}, bf16[1,2048,128]{2,1,0:T(8,128)(2,1)}, u32[]{:S(2)}) copy-start(bf16[1,2048,128]{2,1,0:T(8,128)(2,1)} %param.30) | copy-start | bytes 1572868
  19.5 23.0 %copy-start.6 = (bf16[512,2,128]{2,1,0:T(2,128)(2,1)S(1)}, bf16[512,2,128]{2,1,0:T(2,128)(2,1)}, u32[]{:S(2)}) copy-start(bf16[512,2,128]{2,1,0:T(2,128)(2,1)} %param.18) | copy-start | bytes 786436
  19.5 36.9 %all-to-all-start = ((bf16[4,96,2048]{2,1,0:T(8,128)(2,1)}), bf16[4,96,2048]{2,1,0:T(8,128)(2,1)S(1)}, u32[]{:S(2)}, u32[]{:S(2)}) async-start(bf16[4,96,2048]{2,1,0:T(8,128)(2,1)} %bitcast.145), calls=%async_computation.1 | async-start | bytes 3145728 | tf_op jit(solution)/shard_map/all_to_all | solution.py:141
  24.8 198.9 %reduce-scatter.2.cloned.1.call-start = ((), (), s32[]{:S(2)}) async-start(), calls=%async_computation.5 | async-start | bytes 2359296 | tf_op jit(solution)/shard_map/reduce_scatter | solution.py:107
  24.8 14.1 %collective-permute-start = (bf16[1,2048,128]{2,1,0:T(8,128)(2,1)S(1)}, bf16[1,2048,128]{2,1,0:T(8,128)(2,1)}, u32[]{:S(2)}, u32[]{:S(2)}) collective-permute-start(bf16[1,2048,128]{2,1,0:T(8,128)(2,1)S(1)} %copy-done.5), channel_id=1, source_target_pairs={{0,1},{1,2},{2,3},{3,4},{4,5},{5,6},{6,7},{7,0},{8,9},{9,10},{10,1... | collective-permute-start | bytes 1572872 | tf_op jit(solution)/shard_map/ppermute | solution.py:14
  24.9 14.0 %collective-permute-start.1 = (bf16[1,2048,128]{2,1,0:T(8,128)(2,1)S(1)}, bf16[1,2048,128]{2,1,0:T(8,128)(2,1)}, u32[]{:S(2)}, u32[]{:S(2)}) collective-permute-start(bf16[1,2048,128]{2,1,0:T(8,128)(2,1)S(1)} %copy-done.5), channel_id=1, source_target_pairs={{1,0},{2,1},{3,2},{4,3},{5,4},{6,5},{7,6},{0,7},{9,8},{10,9},{11,1... | collective-permute-start | bytes 1572872 | tf_op jit(solution)/shard_map/ppermute | solution.py:14
  38.9 13.9 %collective-permute-start.2 = (bf16[1,2048,128]{2,1,0:T(8,128)(2,1)}, bf16[1,2048,128]{2,1,0:T(8,128)(2,1)}, u32[]{:S(2)}, u32[]{:S(2)}) collective-permute-start(bf16[1,2048,128]{2,1,0:T(8,128)(2,1)} %collective-permute-done), channel_id=1, source_target_pairs={{0,1},{1,2},{2,3},{3,4},{4,5},{5,6},{6,7},{7,0},{8,9},{9,10},{10,1... | collective-permute-start | bytes 1572872 | tf_op jit(solution)/shard_map/ppermute | solution.py:29
  38.9 13.9 %collective-permute-start.3 = (bf16[1,2048,128]{2,1,0:T(8,128)(2,1)}, bf16[1,2048,128]{2,1,0:T(8,128)(2,1)}, u32[]{:S(2)}, u32[]{:S(2)}) collective-permute-start(bf16[1,2048,128]{2,1,0:T(8,128)(2,1)} %collective-permute-done.1), channel_id=1, source_target_pairs={{1,0},{2,1},{3,2},{4,3},{5,4},{6,5},{7,6},{0,7},{9,8},{10,9},{11,1... | collective-permute-start | bytes 1572872 | tf_op jit(solution)/shard_map/ppermute | solution.py:29
  52.8 53.6 %collective-permute-start.4 = (bf16[1,2048,128]{2,1,0:T(8,128)(2,1)}, bf16[1,2048,128]{2,1,0:T(8,128)(2,1)}, u32[]{:S(2)}, u32[]{:S(2)}) collective-permute-start(bf16[1,2048,128]{2,1,0:T(8,128)(2,1)} %collective-permute-done.2), channel_id=1, source_target_pairs={{0,1},{1,2},{2,3},{3,4},{4,5},{5,6},{6,7},{7,0},{8,9},{9,10},{10,1... | collective-permute-start | bytes 1572872 | tf_op jit(solution)/shard_map/ppermute | solution.py:29
  52.8 55.9 %collective-permute-start.5 = (bf16[1,2048,128]{2,1,0:T(8,128)(2,1)}, bf16[1,2048,128]{2,1,0:T(8,128)(2,1)}, u32[]{:S(2)}, u32[]{:S(2)}) collective-permute-start(bf16[1,2048,128]{2,1,0:T(8,128)(2,1)} %collective-permute-done.3), channel_id=1, source_target_pairs={{1,0},{2,1},{3,2},{4,3},{5,4},{6,5},{7,6},{0,7},{9,8},{10,9},{11,1... | collective-permute-start | bytes 1572872 | tf_op jit(solution)/shard_map/ppermute | solution.py:29
  79.3 3.2 %copy-start.7 = (bf16[512,2,128]{0,2,1:T(8,128)(2,1)S(1)}, bf16[512,2,128]{0,2,1:T(8,128)(2,1)}, u32[]{:S(2)}) copy-start(bf16[512,2,128]{0,2,1:T(8,128)(2,1)} %copy.27) | copy-start | bytes 786436
  82.5 11.0 %copy-start.11 = (f32[2]{0:T(128)S(1)}, f32[2]{0:T(128)}, u32[]{:S(2)}) copy-start(f32[2]{0:T(128)} %param.21) | copy-start | bytes 28
  86.6 1.1 copy-start.1
  86.6 1.5 copy-start.3
  88.8 0.8 copy-start.2
  93.5 1.6 copy-start.12
  106.4 21.7 %collective-permute-start.6 = (bf16[1,2048,128]{2,1,0:T(8,128)(2,1)}, bf16[1,2048,128]{2,1,0:T(8,128)(2,1)S(1)}, u32[]{:S(2)}, u32[]{:S(2)}) collective-permute-start(bf16[1,2048,128]{2,1,0:T(8,128)(2,1)} %collective-permute-done.4), channel_id=1, source_target_pairs={{0,1},{1,2},{2,3},{3,4},{4,5},{5,6},{6,7},{7,0},{8,9},{9,10},{10,1... | collective-permute-start | bytes 1572872 | tf_op jit(solution)/shard_map/ppermute | solution.py:29
  188.9 3.8 %copy-start.10 = (f32[128,2]{0,1:T(2,128)S(1)}, f32[128,2]{0,1:T(2,128)}, u32[]{:S(2)}) copy-start(f32[128,2]{0,1:T(2,128)} %param.28) | copy-start | bytes 3076
  188.9 3.8 %copy-start.13 = (f32[128]{0:T(128)S(1)}, f32[128]{0:T(128)}, u32[]{:S(2)}) copy-start(f32[128]{0:T(128)} %param.27) | copy-start | bytes 1540
  188.9 23.6 %all-to-all-start.1 = ((bf16[4,96,2048]{2,1,0:T(8,128)(2,1)}), bf16[4,96,2048]{2,1,0:T(8,128)(2,1)S(1)}, u32[]{:S(2)}, u32[]{:S(2)}) async-start(bf16[4,96,2048]{2,1,0:T(8,128)(2,1)} %bitcast.146), calls=%async_computation.2 | async-start | bytes 3145728 | tf_op jit(solution)/shard_map/all_to_all | solution.py:168
Sparse Core Ops, SparseCore 0:
  10.4 37.6 all-gather.4
  50.6 28.6 all-gather.6
  80.9 53.3 all-gather.10
  135.7 44.5 all-gather.8
  183.0 34.2 reduce-scatter.1
